TPU v7x, 256 devices: a whole 4x4x8 slice. The times are simulated.
256 devices in a mesh: sp: 16 (over y, x), tp: 16 (over z, core).
Axes of the slice: x: 4, y: 4, z: 8, core: 2. Of those that a mesh axis runs over, the one named last changes fastest.
Arguments:
- queries: bfloat16 [8192, 2048], P('sp', 'tp'), may hold values from -16 to 16
- key_vectors: bfloat16 [8192, 2048], P('sp', 'tp'), may hold values from -4 to 4
- value_vectors: bfloat16 [8192, 2048], P('sp', 'tp'), may hold values from -5 to 5
- forget_totals: float32 [8192, 16], P('sp', 'tp'), may hold values from -1368 to 0, as said below
- head_gain: float32 [2048], P('tp'), may hold values from 0.1 to 1.9
- stream: bfloat16 [8192, 2048], P(('sp', 'tp')), may hold values from -6 to 6
- out_weight: bfloat16 [2048, 2048], replicated, may hold values from -0.125 to 0.125
- norm_gain: float32 [2048], replicated, may hold values from 0.1 to 1.9
- routing: int32 [8192, 2], P(('sp', 'tp')), may hold values from 0 to 15, all different within a row; in each aligned block of 32 rows (0 to 31, 32 to 63, ...) at most 8 rows name the same one
- route_weights: float32 [8192, 2], P(('sp', 'tp')), may hold values from 0.2 to 1
- gate_weight: bfloat16 [16, 2048, 4096], P('sp', None, 'tp'), may hold values from -0.125 to 0.125
- up_weight: bfloat16 [16, 2048, 4096], P('sp', None, 'tp'), may hold values from -0.125 to 0.125
- down_weight: bfloat16 [16, 4096, 2048], P('sp', 'tp'), may hold values from -0.09375 to 0.09375
Outputs:
- layer_out: bfloat16 [8192, 2048], P(('sp', 'tp'))
Inputs may be any that keep to these rules, and one draw needn't show every extreme that they name: `forget_totals`: along the positions, the values of each head never rise. `routing`: A token's 2 experts differ. Within the tokens of one device (aligned blocks of 32 rows) no expert is named more than 8 times.
All inputs are finite; a program needn't handle non-finite values.
Results may differ from a plain program's by a relative error of at most 0.01145.
Values may be sent and summed in bfloat16 or wider, within the bound.
A program may use at most 128 MiB of HBM per device.

v0:
```python
from functools import partial
import jax
import jax.numpy as jnp
from jax import lax
from jax.sharding import PartitionSpec as P

HD = 128
TOP = 2
masked_score = -1e30


def sent_together(arrays, axis, dim, along):
    ends, at = ([], 0)
    for a in arrays[:-1]:
        at += a.shape[along]
        ends.append(at)
    both = jnp.concatenate(arrays, axis=along)
    return tuple(jnp.split(lax.all_gather(both, axis, axis=dim, tiled=True), ends, axis=along))


def attend_block(
    totals, query_rows, query_gate, query_pos, key_rows, value_rows, key_gate, key_pos
):
    run_max, run_sum, run_acc = totals
    scores = jnp.einsum("qhd,khd->hqk", query_rows, key_rows, preferred_element_type=jnp.float32)
    scores = scores * HD ** (-0.5) + query_gate[:, :, None] - key_gate[:, None, :]
    visible = (key_pos[None, :] <= query_pos[:, None])[None]
    scores = jnp.where(visible, scores, masked_score)
    new_max = jnp.maximum(run_max, jnp.max(scores, axis=2))
    lifted = jnp.where(visible, jnp.exp(scores - new_max[:, :, None]), 0.0)
    rescale = jnp.exp(run_max - new_max)
    new_sum = run_sum * rescale + jnp.sum(lifted, axis=2)
    product = jnp.einsum(
        "hqk,khd->hqd", lifted.astype(jnp.bfloat16), value_rows, preferred_element_type=jnp.float32
    )
    new_acc = run_acc * rescale[:, :, None] + product
    return (new_max, new_sum, new_acc)


def keep_totals(totals_in):
    return totals_in


def make_folder(segments, gathered_gates):

    def fold_keys(state_all, key_piece, first_key):
        key_part, value_part = key_piece
        key_total = key_part.shape[0]
        block_len = min(512, key_total)
        heads_dev = segments[0][0].shape[1]
        key_part = key_part.reshape(key_total, heads_dev, HD)
        value_part = value_part.reshape(key_total, heads_dev, HD)

        def one_block(block_index, state_now):
            offset = block_index * block_len
            key_rows = lax.dynamic_slice_in_dim(key_part, offset, block_len, 0)
            value_rows = lax.dynamic_slice_in_dim(value_part, offset, block_len, 0)
            key_pos = offset + jnp.arange(block_len, dtype=jnp.int32)
            key_gate = jnp.transpose(lax.dynamic_slice_in_dim(gathered_gates, offset, block_len, 0))
            updated = []
            for segment, totals_in in zip(segments, state_now):
                query_rows, query_gate, query_pos = segment
                needed = offset <= query_pos[-1]
                advance = partial(
                    attend_block,
                    query_rows=query_rows,
                    query_gate=query_gate,
                    query_pos=query_pos,
                    key_rows=key_rows,
                    value_rows=value_rows,
                    key_gate=key_gate,
                    key_pos=key_pos,
                )
                updated.append(lax.cond(needed, advance, keep_totals, totals_in))
            return tuple(updated)

        return lax.fori_loop(0, key_total // block_len, one_block, state_all)

    return fold_keys


def on_device(
    queries,
    key_vectors,
    value_vectors,
    forget_totals,
    head_gain,
    stream,
    out_weight,
    norm_gain,
    routing,
    route_weights,
    gate_weight,
    up_weight,
    down_weight,
):
    tok_count = queries.shape[0]
    heads_dev = queries.shape[1] // HD
    sp_index = lax.axis_index("sp")
    sp_count = lax.axis_size("sp")
    gathered_gates = lax.all_gather(forget_totals, "sp", axis=0, tiled=True)
    first_pos = sp_index * tok_count
    query_pos = first_pos + jnp.arange(tok_count, dtype=jnp.int32)
    query_gate = jnp.transpose(lax.dynamic_slice_in_dim(gathered_gates, first_pos, tok_count, 0))
    segments = [(queries.reshape(tok_count, heads_dev, HD), query_gate, query_pos)]
    starting = (
        (
            jnp.full((heads_dev, tok_count), masked_score, jnp.float32),
            jnp.zeros((heads_dev, tok_count), jnp.float32),
            jnp.zeros((heads_dev, tok_count, HD), jnp.float32),
        ),
    )
    folder = make_folder(segments, gathered_gates)
    totals = folder(starting, sent_together((key_vectors, value_vectors), "sp", 0, 1), jnp.int32(0))
    run_max, run_sum, run_acc = totals[0]
    attended = run_acc / run_sum[:, :, None]
    inverse_rms = lax.rsqrt(jnp.mean(attended * attended, axis=2, keepdims=True) + 1e-06)
    normed = attended * inverse_rms * head_gain.reshape(heads_dev, 1, HD)
    head_out = (
        jnp.transpose(normed, (1, 0, 2)).reshape(tok_count, heads_dev * HD).astype(jnp.bfloat16)
    )
    token_heads = lax.all_to_all(head_out, "tp", split_axis=0, concat_axis=1, tiled=True)
    mixed_rows = jnp.dot(token_heads, out_weight, preferred_element_type=jnp.float32)
    resid_sum = stream.astype(jnp.float32) + mixed_rows
    center = resid_sum - jnp.mean(resid_sum, axis=1, keepdims=True)
    normed_rows = (
        center * lax.rsqrt(jnp.mean(center * center, axis=1, keepdims=True) + 1e-05) * norm_gain
    ).astype(jnp.bfloat16)
    row_count = normed_rows.shape[0]
    capacity = max(2, 2 * TOP * row_count // sp_count)
    flat_expert = routing.reshape(-1)
    onehot = (flat_expert[:, None] == jnp.arange(sp_count, dtype=jnp.int32)[None, :]).astype(
        jnp.int32
    )
    earlier = jnp.cumsum(onehot, axis=0) - onehot
    slot_index = flat_expert * capacity + jnp.sum(earlier * onehot, axis=1)
    slot_grid = slot_index.reshape(row_count, TOP)
    slot_ids = jnp.arange(sp_count * capacity, dtype=jnp.int32)
    placing = jnp.sum(
        (slot_grid[None, :, :] == slot_ids[:, None, None]).astype(jnp.float32), axis=2
    ).astype(jnp.bfloat16)
    outgoing = jnp.dot(placing, normed_rows, preferred_element_type=jnp.float32).astype(
        jnp.bfloat16
    )
    outgoing = outgoing.reshape(sp_count, capacity, normed_rows.shape[1])
    arrived = lax.all_to_all(outgoing, "sp", split_axis=0, concat_axis=0, tiled=True)
    row_piece = lax.all_gather(arrived.reshape(-1, arrived.shape[2]), "tp", axis=0, tiled=True)
    gate_pre = jnp.dot(row_piece, gate_weight[0], preferred_element_type=jnp.float32)
    up_pre = jnp.dot(row_piece, up_weight[0], preferred_element_type=jnp.float32)
    hidden = (jax.nn.silu(gate_pre) * up_pre).astype(jnp.bfloat16)
    summed = lax.psum_scatter(
        jnp.dot(hidden, down_weight[0], preferred_element_type=jnp.float32).astype(jnp.bfloat16),
        "tp",
        scatter_dimension=0,
        tiled=True,
    )
    expert_out = summed.reshape(sp_count, capacity, -1)
    returned = lax.all_to_all(expert_out, "sp", split_axis=0, concat_axis=0, tiled=True)
    picked = returned.reshape(sp_count * capacity, -1)[slot_index].astype(jnp.float32)
    weighted = picked * route_weights.reshape(-1)[:, None]
    routed = jnp.sum(weighted.reshape(row_count, TOP, -1), axis=1)
    return (resid_sum + routed).astype(jnp.bfloat16)


def solution(mesh):
    in_specs = (
        P("sp", "tp"),
        P("sp", "tp"),
        P("sp", "tp"),
        P("sp", "tp"),
        P("tp"),
        P(("sp", "tp"), None),
        P(),
        P(),
        P(("sp", "tp"), None),
        P(("sp", "tp"), None),
        P("sp", None, "tp"),
        P("sp", None, "tp"),
        P("sp", "tp", None),
    )
    out_specs = P(("sp", "tp"), None)
    return jax.shard_map(
        on_device, mesh=mesh, in_specs=in_specs, out_specs=out_specs, check_vma=False
    )
```

profile of v0, /device:TPU:2, one launch (start us, length us, event | category | flops | bytes accessed | tf_op | source)
XLA Modules:
  0.0 334.1 jit_solution(2829663943095619503)
XLA Ops:
  6.5 1.8 pad_maximum_fusion
  8.3 0.8 copy.26
  9.7 23.4 %all_gather.10 = f32[8192,1]{0,1:T(1,128)S(1)} all-gather(f32[512,1]{0,1:T(1,128)} %param.20), channel_id=1, replica_groups=mesh['sp'=16,'tp'=16] {'sp'}, dimensions={0}, use_global_device_ids=true | all-gather | bytes 34816 | tf_op jit(solution)/shard_map/all_gather | solution.py:101
  33.1 36.1 %all-gather.3.cloned.1.call-done = bf16[8192,256]{1,0:T(8,128)(2,1)} async-done(((bf16[512,256]{1,0:T(8,128)(2,1)}), bf16[8192,256]{1,0:T(8,128)(2,1)}) %all-gather.3.cloned.1.call-update) | async-done | bytes 4194320 | tf_op jit(solution)/shard_map/all_gather | solution.py:18
  69.2 3.8 %slice_bitcast_fusion = (bf16[8192,1,128]{2,0,1:T(8,128)(2,1)S(1)}, bf16[8192,1,128]{2,0,1:T(8,128)(2,1)}) fusion(bf16[8192,256]{1,0:T(8,128)(2,1)} %all-gather.3.cloned.1.call-done), kind=kLoop, calls=%fused_computation.33 | loop fusion | bytes 8388608 | tf_op jit(solution)/shard_map/reshape | solution.py:52
  73.1 23.5 %while.17 = (s32[]{:T(128)}, f32[1,512]{1,0:T(1,128)S(1)}, f32[1,512]{1,0:T(1,128)S(1)}, f32[1,512,128]{2,1,0:T(8,128)S(1)}, s32[512]{0:T(512)S(1)}, /*index=5*/...) while((s32[]{:T(128)}, f32[1,512]{1,0:T(1,128)S(1)}, ...), condition=%wide.region_5.6_spmd, body=%wide.region_0.5_spmd.sunk | while | flops 138020352 | bytes 4122969 | solution.py:77
  74.3 2.2 conditional.2
  74.3 1.4 fusion.38
  77.7 2.2 conditional.2
  77.7 1.4 fusion.38
  96.8 0.9 multiply_convert_fusion.1
  97.7 7.1 %all-to-all-start = ((bf16[16,32,128]{2,1,0:T(8,128)(2,1)}), bf16[16,32,128]{2,1,0:T(8,128)(2,1)S(1)}, u32[]{:S(2)}, u32[]{:S(2)}) async-start(bf16[16,32,128]{2,1,0:T(8,128)(2,1)} %bitcast.16), calls=%async_computation | async-start | bytes 262144 | tf_op jit(solution)/shard_map/all_to_all | solution.py:122
  105.1 8.4 %all-to-all-done = bf16[16,32,128]{2,1,0:T(8,128)(2,1)S(1)} async-done(((bf16[16,32,128]{2,1,0:T(8,128)(2,1)}), bf16[16,32,128]{2,1,0:T(8,128)(2,1)S(1)}, u32[]{:S(2)}, u32[]{:S(2)}) %all-to-all-start) | async-done | bytes 131104 | tf_op jit(solution)/shard_map/all_to_all | solution.py:122
  113.5 5.0 %fusion.39 = (f32[32]{0:T(128)S(1)}, f32[32,2048]{1,0:T(8,128)S(1)}) fusion(bf16[2048,2048]{1,0:T(8,128)(2,1)} %param.23, bf16[32,2048]{1,0:T(8,128)(2,1)} %param.22, bf16[16,32,128]{2,1,0:T(8,128)(2,1)S(1)} %all-to-all-done), kind=kOutput, calls=%fused_computation.72 | convolution fusion | flops 268632032 | bytes 8913024 | tf_op jit(solution)/shard_map/dot_general | solution.py:123
  119.1 46.6 %all_to_all.26 = bf16[16,8,2048]{2,1,0:T(8,128)(2,1)} all-to-all(bf16[16,8,2048]{2,1,0:T(8,128)(2,1)S(1)} %fusion.21), channel_id=1, replica_groups=mesh['sp'=16,'tp'=16] {'sp'}, dimensions={0} | all-to-all | bytes 1048576 | tf_op jit(solution)/shard_map/all_to_all | solution.py:146
  165.8 49.9 %all-gather.5.cloned.1.call-done = bf16[2048,2048]{1,0:T(8,128)(2,1)} async-done(((bf16[128,2048]{1,0:T(8,128)(2,1)}), bf16[2048,2048]{1,0:T(8,128)(2,1)}) %all-gather.5.cloned.1.call-update) | async-done | bytes 8388624 | tf_op jit(solution)/shard_map/all_gather | solution.py:147
  215.8 7.1 %fusion.25 = f32[2048,256]{1,0:T(8,128)} fusion(bf16[2048,2048]{1,0:T(8,128)(2,1)} %all-gather.5.cloned.1.call-done, bf16[1,2048,256]{2,1,0:T(8,128)(2,1)S(1)} %copy-done.4), kind=kOutput, calls=%fused_computation.37 | convolution fusion | flops 2147483648 | bytes 11534336 | tf_op jit(solution)/shard_map/dot_general | solution.py:148
  222.9 16.8 %convolution_convert_fusion = bf16[2048,2048]{1,0:T(8,128)(2,1)} fusion(bf16[2048,2048]{1,0:T(8,128)(2,1)} %all-gather.5.cloned.1.call-done, f32[2048,256]{1,0:T(8,128)} %fusion.25, bf16[1,256,2048]{2,1,0:T(8,128)(2,1)S(1)} %copy-done, bf16[1,2048,256]{2,1,0:T(8,128)(2,1)} %param.28), kind=kOutput, calls=%fused_computation.27 | convolution fusion | flops 4302307328 | bytes 20971520 | tf_op jit(solution)/shard_map/dot_general | solution.py:152
  239.7 69.3 %reduce-scatter.2.cloned.1.call-done = bf16[128,2048]{1,0:T(8,128)(2,1)} async-done(((bf16[2048,2048]{1,0:T(8,128)(2,1)}), bf16[128,2048]{1,0:T(8,128)(2,1)}) %reduce-scatter.2.cloned.1.call-update) | async-done | bytes 524304 | tf_op jit(solution)/shard_map/reduce_scatter | solution.py:151
  309.0 7.3 %all-to-all-start.2 = ((bf16[16,8,2048]{2,1,0:T(8,128)(2,1)}), bf16[16,8,2048]{2,1,0:T(8,128)(2,1)S(1)}, u32[]{:S(2)}, u32[]{:S(2)}) async-start(bf16[16,8,2048]{2,1,0:T(8,128)(2,1)} %bitcast.76), calls=%async_computation.3 | async-start | bytes 1048576 | tf_op jit(solution)/shard_map/all_to_all | solution.py:158
  316.5 8.6 %all-to-all-done.2 = bf16[16,8,2048]{2,1,0:T(8,128)(2,1)S(1)} async-done(((bf16[16,8,2048]{2,1,0:T(8,128)(2,1)}), bf16[16,8,2048]{2,1,0:T(8,128)(2,1)S(1)}, u32[]{:S(2)}, u32[]{:S(2)}) %all-to-all-start.2) | async-done | bytes 524320 | tf_op jit(solution)/shard_map/all_to_all | solution.py:158
  325.1 0.7 gather_fusion
  326.2 0.7 multiply_reduce_fusion
  326.9 0.7 add_convert_fusion
  (100 shorter events, 13.3 us)
Async XLA Ops:
  6.5 216.3 %copy-start = (bf16[1,256,2048]{2,1,0:T(8,128)(2,1)S(1)}, bf16[1,256,2048]{2,1,0:T(8,128)(2,1)}, u32[]{:S(2)}) copy-start(bf16[1,256,2048]{2,1,0:T(8,128)(2,1)} %param.29) | copy-start | bytes 3145732
  6.5 62.7 %all-gather.3.cloned.1.call-start = ((), (), s32[]{:S(2)}) async-start(), calls=%async_computation.4 | async-start | bytes 4456448 | tf_op jit(solution)/shard_map/all_gather | solution.py:18
  73.1 23.8 %copy-start.3 = (f32[128]{0:T(128)S(1)}, f32[128]{0:T(128)}, u32[]{:S(2)}) copy-start(f32[128]{0:T(128)} %param.21) | copy-start | bytes 1540
  97.7 15.8 %all-to-all-start = ((bf16[16,32,128]{2,1,0:T(8,128)(2,1)}), bf16[16,32,128]{2,1,0:T(8,128)(2,1)S(1)}, u32[]{:S(2)}, u32[]{:S(2)}) async-start(bf16[16,32,128]{2,1,0:T(8,128)(2,1)} %bitcast.16), calls=%async_computation | async-start | bytes 262144 | tf_op jit(solution)/shard_map/all_to_all | solution.py:122
  104.8 110.9 %all-gather.5.cloned.1.call-start = ((), (), s32[]{:S(2)}) async-start(), calls=%async_computation.5 | async-start | bytes 8912896 | tf_op jit(solution)/shard_map/all_gather | solution.py:147
  105.1 13.7 %copy-start.1 = (f32[2048]{0:T(1024)S(1)}, f32[2048]{0:T(1024)}, u32[]{:S(2)}) copy-start(f32[2048]{0:T(1024)} %param.24) | copy-start | bytes 24580
  118.5 97.3 %copy-start.4 = (bf16[1,2048,256]{2,1,0:T(8,128)(2,1)S(1)}, bf16[1,2048,256]{2,1,0:T(8,128)(2,1)}, u32[]{:S(2)}) copy-start(bf16[1,2048,256]{2,1,0:T(8,128)(2,1)} %param.27) | copy-start | bytes 3145732
  165.8 143.2 %reduce-scatter.2.cloned.1.call-start = ((), (), s32[]{:S(2)}) async-start(), calls=%async_computation.6 | async-start | bytes 8912896 | tf_op jit(solution)/shard_map/reduce_scatter | solution.py:151
  239.7 76.8 %copy-start.2 = (f32[32,2]{0,1:T(2,128)S(1)}, f32[32,2]{0,1:T(2,128)}, u32[]{:S(2)}) copy-start(f32[32,2]{0,1:T(2,128)} %param.26) | copy-start | bytes 772
  309.0 16.1 %all-to-all-start.2 = ((bf16[16,8,2048]{2,1,0:T(8,128)(2,1)}), bf16[16,8,2048]{2,1,0:T(8,128)(2,1)S(1)}, u32[]{:S(2)}, u32[]{:S(2)}) async-start(bf16[16,8,2048]{2,1,0:T(8,128)(2,1)} %bitcast.76), calls=%async_computation.3 | async-start | bytes 1048576 | tf_op jit(solution)/shard_map/all_to_all | solution.py:158
Sparse Core Ops, SparseCore 0:
  9.8 59.4 all-gather.2
  165.9 49.8 all-gather.4
  239.8 69.1 reduce-scatter.1
where the time goes:
time: 335 us; the launch traced here: 334 us
  waiting for transfers between devices  172 us (51%)
  blocking collectives  70.1 us (21%)
  matrix products  33 us (10%)
  local copies, waits for them, and re-layouts  15.5 us (5%)
  starting transfers between devices  14.5 us (4%)
  between operations  13.3 us (4%)
  loops' own time  9.92 us (3%)
  other arithmetic  5.49 us (2%)
    reduce_scatter x1, waiting for transfers between devices, on_device(): lax.psum_scatter(jnp.dot(hidden, down_weight[0], preferred_element_type=j...  69.3 us
    all_gather x1, waiting for transfers between devices, on_device(): lax.all_gather(arrived.reshape(-1, arrived.shape[2]), 'tp', axis=0, tiled...  49.9 us
    all_to_all x1, blocking collectives, on_device(): lax.all_to_all(outgoing, 'sp', split_axis=0, concat_axis=0, tiled=True)  46.6 us
    all_gather x1, waiting for transfers between devices, sent_together(): lax.all_gather(both, axis, axis=dim, tiled=True)  36.1 us
    all_gather x1, blocking collectives, on_device(): gathered_gates = lax.all_gather(forget_totals, 'sp', axis=0, tiled=True)  23.4 us
    dot_general x1, matrix products, on_device(): jnp.dot(hidden, down_weight[0], preferred_element_type=jnp.float32)  16.8 us
    another operation x1, loops' own time, fold_keys(): return lax.fori_loop(0, key_total // block_len, one_block, state_all)  9.6 us
    slice x16, local copies, waits for them, and re-layouts, one_block(): needed = offset <= query_pos[-1]  9.2 us
  transfers between devices with their start and end apart: 5, of which 5 were waited for; matrix products, arithmetic and copies ran while one was open for 1% of the time, Pallas kernels for 0%

commit v1 on v0

--- a/solution.py
+++ b/solution.py
@@ -144,7 +144,12 @@
     )
     outgoing = outgoing.reshape(sp_count, capacity, normed_rows.shape[1])
     arrived = lax.all_to_all(outgoing, "sp", split_axis=0, concat_axis=0, tiled=True)
-    row_piece = lax.all_gather(arrived.reshape(-1, arrived.shape[2]), "tp", axis=0, tiled=True)
+    row_piece = jnp.concatenate(
+        lax.all_to_all(
+            jnp.stack([arrived.reshape(-1, arrived.shape[2])] * lax.axis_size("tp")), "tp", 0, 0
+        ),
+        axis=0,
+    )
     gate_pre = jnp.dot(row_piece, gate_weight[0], preferred_element_type=jnp.float32)
     up_pre = jnp.dot(row_piece, up_weight[0], preferred_element_type=jnp.float32)
     hidden = (jax.nn.silu(gate_pre) * up_pre).astype(jnp.bfloat16)

time: 335 us -> 471 us (1.41)
  blocking collectives: 70.1 us -> 257 us
  waiting for transfers between devices: 172 us -> 120 us
    all_to_all x0 -> x1, blocking collectives: none -> 187 us  [on_device(): lax.all_to_all(jnp.stack([arrived.reshape(-1, arrived.shape[2])] * lax.ax...]
    all_gather x1 -> x0, waiting for transfers between devices: 49.9 us -> none  [on_device(): lax.all_gather(arrived.reshape(-1, arrived.shape[2]), 'tp', axis=0, tiled...]
  transfers between devices with their start and end apart: 5 -> 4, of which waited for: 5 -> 4; matrix products, arithmetic and copies ran while one was open for 1% -> 0% of each run, Pallas kernels for 0% -> 0%
where the time goes in v1:
time: 471 us; the launch traced here: 470 us
  blocking collectives  257 us (55%)
  waiting for transfers between devices  120 us (25%)
  matrix products  29.8 us (6%)
  local copies, waits for them, and re-layouts  19.7 us (4%)
  starting transfers between devices  14.5 us (3%)
  between operations  13.6 us (3%)
  loops' own time  9.92 us (2%)
  other arithmetic  5.5 us (1%)
    all_to_all x1, blocking collectives, on_device(): lax.all_to_all(jnp.stack([arrived.reshape(-1, arrived.shape[2])] * lax.ax...  187 us
    reduce_scatter x1, waiting for transfers between devices, on_device(): lax.psum_scatter(jnp.dot(hidden, down_weight[0], preferred_element_type=j...  66.7 us
    all_to_all x1, blocking collectives, on_device(): lax.all_to_all(outgoing, 'sp', split_axis=0, concat_axis=0, tiled=True)  46.6 us
    all_gather x1, waiting for transfers between devices, sent_together(): lax.all_gather(both, axis, axis=dim, tiled=True)  36.1 us
    all_gather x1, blocking collectives, on_device(): gathered_gates = lax.all_gather(forget_totals, 'sp', axis=0, tiled=True)  23.4 us
    dot_general x1, matrix products, on_device(): jnp.dot(hidden, down_weight[0], preferred_element_type=jnp.float32)  16.8 us
    another operation x1, loops' own time, fold_keys(): return lax.fori_loop(0, key_total // block_len, one_block, state_all)  9.6 us
  transfers between devices with their start and end apart: 4, of which 4 were waited for; matrix products, arithmetic and copies ran while one was open for 0% of the time, Pallas kernels for 0%

profile of v1, /device:TPU:2, one launch (start us, length us, event | category | flops | bytes accessed | tf_op | source)
XLA Modules:
  0.0 469.9 jit_solution(1481307971937641133)
XLA Ops:
  6.5 1.8 pad_maximum_fusion
  8.3 0.8 copy.26
  9.7 23.4 %all_gather.7 = f32[8192,1]{0,1:T(1,128)S(1)} all-gather(f32[512,1]{0,1:T(1,128)} %param.20), channel_id=1, replica_groups=mesh['sp'=16,'tp'=16] {'sp'}, dimensions={0}, use_global_device_ids=true | all-gather | bytes 34816 | tf_op jit(solution)/shard_map/all_gather | solution.py:101
  33.1 36.1 %all-gather.2.cloned.1.call-done = bf16[8192,256]{1,0:T(8,128)(2,1)} async-done(((bf16[512,256]{1,0:T(8,128)(2,1)}), bf16[8192,256]{1,0:T(8,128)(2,1)}) %all-gather.2.cloned.1.call-update) | async-done | bytes 4194320 | tf_op jit(solution)/shard_map/all_gather | solution.py:18
  69.2 3.8 slice_bitcast_fusion
  73.1 23.5 %while.17 = (s32[]{:T(128)}, f32[1,512]{1,0:T(1,128)S(1)}, f32[1,512]{1,0:T(1,128)S(1)}, f32[1,512,128]{2,1,0:T(8,128)S(1)}, s32[512]{0:T(512)S(1)}, /*index=5*/...) while((s32[]{:T(128)}, f32[1,512]{1,0:T(1,128)S(1)}, ...), condition=%wide.region_5.6_spmd, body=%wide.region_0.5_spmd.sunk | while | flops 138020352 | bytes 4122969 | solution.py:77
  74.3 2.2 conditional.2
  74.3 1.4 fusion.38
  77.7 2.2 conditional.2
  77.7 1.4 fusion.38
  96.8 0.9 multiply_convert_fusion.1
  97.7 7.1 %all-to-all-start = ((bf16[16,32,128]{2,1,0:T(8,128)(2,1)}), bf16[16,32,128]{2,1,0:T(8,128)(2,1)S(1)}, u32[]{:S(2)}, u32[]{:S(2)}) async-start(bf16[16,32,128]{2,1,0:T(8,128)(2,1)} %bitcast.16), calls=%async_computation | async-start | bytes 262144 | tf_op jit(solution)/shard_map/all_to_all | solution.py:122
  105.1 8.4 %all-to-all-done = bf16[16,32,128]{2,1,0:T(8,128)(2,1)S(1)} async-done(((bf16[16,32,128]{2,1,0:T(8,128)(2,1)}), bf16[16,32,128]{2,1,0:T(8,128)(2,1)S(1)}, u32[]{:S(2)}, u32[]{:S(2)}) %all-to-all-start) | async-done | bytes 131104 | tf_op jit(solution)/shard_map/all_to_all | solution.py:122
  113.5 5.0 %fusion.39 = (f32[32]{0:T(128)S(1)}, f32[32,2048]{1,0:T(8,128)S(1)}) fusion(bf16[2048,2048]{1,0:T(8,128)(2,1)} %param.23, bf16[32,2048]{1,0:T(8,128)(2,1)} %param.22, bf16[16,32,128]{2,1,0:T(8,128)(2,1)S(1)} %all-to-all-done), kind=kOutput, calls=%fused_computation.72 | convolution fusion | flops 268632032 | bytes 8913024 | tf_op jit(solution)/shard_map/dot_general | solution.py:123
  119.1 46.6 %all_to_all.31 = bf16[16,8,2048]{2,1,0:T(8,128)(2,1)S(1)} all-to-all(bf16[16,8,2048]{2,1,0:T(8,128)(2,1)S(1)} %fusion.21), channel_id=1, replica_groups=mesh['sp'=16,'tp'=16] {'sp'}, dimensions={0} | all-to-all | bytes 1048576 | tf_op jit(solution)/shard_map/all_to_all | solution.py:146
  165.7 1.1 stack.3
  166.7 187.3 %all_to_all.32 = bf16[16,128,2048]{2,1,0:T(8,128)(2,1)S(1)} all-to-all(bf16[16,128,2048]{2,1,0:T(8,128)(2,1)S(1)} %stack.3), channel_id=1, replica_groups=mesh['sp'=16,'tp'=16] {'tp'}, dimensions={0} | all-to-all | bytes 16777216 | tf_op jit(solution)/shard_map/all_to_all | solution.py:148
  354.0 3.2 copy-done.1
  357.2 3.8 fusion.25
  361.0 16.8 %convolution_convert_fusion = bf16[2048,2048]{1,0:T(8,128)(2,1)} fusion(bf16[2048,2048]{1,0:T(8,128)(2,1)} %bitcast.75, f32[2048,256]{1,0:T(8,128)} %fusion.25, bf16[1,256,2048]{2,1,0:T(8,128)(2,1)S(1)} %copy-done, bf16[1,2048,256]{2,1,0:T(8,128)(2,1)} %param.28), kind=kOutput, calls=%fused_computation.27 | convolution fusion | flops 4302307328 | bytes 20971520 | tf_op jit(solution)/shard_map/dot_general | solution.py:157
  377.9 66.7 %reduce-scatter.2.cloned.1.call-done = bf16[128,2048]{1,0:T(8,128)(2,1)} async-done(((bf16[2048,2048]{1,0:T(8,128)(2,1)}), bf16[128,2048]{1,0:T(8,128)(2,1)}) %reduce-scatter.2.cloned.1.call-update) | async-done | bytes 524304 | tf_op jit(solution)/shard_map/reduce_scatter | solution.py:156
  444.5 7.3 %all-to-all-start.3 = ((bf16[16,8,2048]{2,1,0:T(8,128)(2,1)}), bf16[16,8,2048]{2,1,0:T(8,128)(2,1)S(1)}, u32[]{:S(2)}, u32[]{:S(2)}) async-start(bf16[16,8,2048]{2,1,0:T(8,128)(2,1)} %bitcast.79), calls=%async_computation.4 | async-start | bytes 1048576 | tf_op jit(solution)/shard_map/all_to_all | solution.py:163
  452.0 8.6 %all-to-all-done.3 = bf16[16,8,2048]{2,1,0:T(8,128)(2,1)S(1)} async-done(((bf16[16,8,2048]{2,1,0:T(8,128)(2,1)}), bf16[16,8,2048]{2,1,0:T(8,128)(2,1)S(1)}, u32[]{:S(2)}, u32[]{:S(2)}) %all-to-all-start.3) | async-done | bytes 524320 | tf_op jit(solution)/shard_map/all_to_all | solution.py:163
  460.6 0.7 gather_fusion
  (101 shorter events, 14.7 us)
Async XLA Ops:
  6.5 354.5 %copy-start = (bf16[1,256,2048]{2,1,0:T(8,128)(2,1)S(1)}, bf16[1,256,2048]{2,1,0:T(8,128)(2,1)}, u32[]{:S(2)}) copy-start(bf16[1,256,2048]{2,1,0:T(8,128)(2,1)} %param.29) | copy-start | bytes 3145732
  6.5 62.7 %all-gather.2.cloned.1.call-start = ((), (), s32[]{:S(2)}) async-start(), calls=%async_computation.5 | async-start | bytes 4456448 | tf_op jit(solution)/shard_map/all_gather | solution.py:18
  73.1 23.8 %copy-start.4 = (f32[128]{0:T(128)S(1)}, f32[128]{0:T(128)}, u32[]{:S(2)}) copy-start(f32[128]{0:T(128)} %param.21) | copy-start | bytes 1540
  97.7 15.8 %all-to-all-start = ((bf16[16,32,128]{2,1,0:T(8,128)(2,1)}), bf16[16,32,128]{2,1,0:T(8,128)(2,1)S(1)}, u32[]{:S(2)}, u32[]{:S(2)}) async-start(bf16[16,32,128]{2,1,0:T(8,128)(2,1)} %bitcast.16), calls=%async_computation | async-start | bytes 262144 | tf_op jit(solution)/shard_map/all_to_all | solution.py:122
  104.8 339.7 %reduce-scatter.2.cloned.1.call-start = ((), (), s32[]{:S(2)}) async-start(), calls=%async_computation.6 | async-start | bytes 8912896 | tf_op jit(solution)/shard_map/reduce_scatter | solution.py:156
  105.0 13.7 %copy-start.2 = (f32[2048]{0:T(1024)S(1)}, f32[2048]{0:T(1024)}, u32[]{:S(2)}) copy-start(f32[2048]{0:T(1024)} %param.24) | copy-start | bytes 24580
  166.7 190.5 %copy-start.5 = (bf16[1,2048,256]{2,1,0:T(8,128)(2,1)S(1)}, bf16[1,2048,256]{2,1,0:T(8,128)(2,1)}, u32[]{:S(2)}) copy-start(bf16[1,2048,256]{2,1,0:T(8,128)(2,1)} %param.27) | copy-start | bytes 3145732
  354.0 3.2 copy-start.1
  377.9 74.1 %copy-start.3 = (f32[32,2]{0,1:T(2,128)S(1)}, f32[32,2]{0,1:T(2,128)}, u32[]{:S(2)}) copy-start(f32[32,2]{0,1:T(2,128)} %param.26) | copy-start | bytes 772
  444.5 16.1 %all-to-all-start.3 = ((bf16[16,8,2048]{2,1,0:T(8,128)(2,1)}), bf16[16,8,2048]{2,1,0:T(8,128)(2,1)S(1)}, u32[]{:S(2)}, u32[]{:S(2)}) async-start(bf16[16,8,2048]{2,1,0:T(8,128)(2,1)} %bitcast.79), calls=%async_computation.4 | async-start | bytes 1048576 | tf_op jit(solution)/shard_map/all_to_all | solution.py:163
Sparse Core Ops, SparseCore 0:
  9.8 59.4 all-gather.1
  378.0 66.4 reduce-scatter.1
